TPU v7x, 128 devices: a whole 4x4x4 slice. The times are simulated.
128 devices in a mesh: ep: 64 (over z, y, x), tp: 2 (over core).
Axes of the slice: x: 4, y: 4, z: 4, core: 2. Of those that a mesh axis runs over, the one named last changes fastest.
Arguments:
- tokens: bfloat16 [1024, 2048], P('ep'), may hold values from -6 to 6
- norm_attn: float32 [2048], replicated, may hold values from 0.1 to 1.9
- w_query: bfloat16 [2048, 2048], P(None, 'tp'), may hold values from -0.125 to 0.125
- w_key: bfloat16 [2048, 256], P(None, 'tp'), may hold values from -0.125 to 0.125
- w_value: bfloat16 [2048, 256], P(None, 'tp'), may hold values from -0.125 to 0.125
- w_out: bfloat16 [2048, 2048], P('tp'), may hold values from -0.125 to 0.125
- attn_bias: float32 [32], P('tp'), may hold values from -7 to -1
- cache_keys: bfloat16 [1024, 1024, 256], P('ep', None, 'tp'), may hold values from -6 to 6
- cache_values: bfloat16 [1024, 1024, 256], P('ep', None, 'tp'), may hold values from -6 to 6
- lengths: int32 [1024], P('ep'), may hold values from 256 to 1024
- norm_ffn: float32 [2048], replicated, may hold values from 0.1 to 1.9
- expert_gate: bfloat16 [2048, 57344], P(None, ('ep', 'tp')), may hold values from -0.125 to 0.125
- expert_up: bfloat16 [2048, 57344], P(None, ('ep', 'tp')), may hold values from -0.125 to 0.125
- expert_down: bfloat16 [57344, 2048], P(('ep', 'tp')), may hold values from -0.0625 to 0.0625
- dense_gate_w: bfloat16 [2048, 7168], P(None, 'ep'), may hold values from -0.125 to 0.125
- dense_up_w: bfloat16 [2048, 7168], P(None, 'ep'), may hold values from -0.125 to 0.125
- dense_down_w: bfloat16 [7168, 2048], P('ep'), may hold values from -0.0625 to 0.0625
- dense_mix: bfloat16 [2048], replicated, may hold values from -0.125 to 0.125
- routes: int32 [1024, 2], P(('ep', 'tp')), may hold values from 0 to 7, all different within a row; in each aligned block of 8 rows (0 to 7, 8 to 15, ...) at most 3 rows name the same one
- route_weights: bfloat16 [1024, 2], P(('ep', 'tp')), may hold values from 0.19921875 to 1
Outputs:
- layer_out: bfloat16 [1024, 2048], P(('ep', 'tp'))
- new_keys: bfloat16 [1024, 256], P('ep', 'tp')
- new_values: bfloat16 [1024, 256], P('ep', 'tp')
Inputs may be any that keep to these rules, and one draw needn't show every extreme that they name: `routes`: in each aligned block of 8 rows (the rows of one device) no expert is named by more than 3 rows, a bound that some block reaches; a row names 2 different experts.
All inputs are finite; a program needn't handle non-finite values.
Results may differ from a plain program's by a relative error of at most 0.015.
Values may be sent and summed in bfloat16 or wider, within the bound.
A program may use at most 128 MiB of HBM per device.

v0:
```python
import jax
import jax.numpy as jnp
from jax import lax
from jax.sharding import PartitionSpec as P

HEAD_DIM = 64
EXPERTS = 8
TOP = 2


EPSILON = 1e-06


def split_up(shard, dim, count):
    dims = shard.shape
    pieces = shard.reshape(*dims[:dim], count, dims[dim] // count, *dims[dim + 1 :])
    return jnp.moveaxis(pieces, dim, 0)


def sum_at_owner(shard, axis, dim):
    pieces = split_up(shard, dim, lax.axis_size(axis))
    arrived = lax.all_to_all(pieces, axis, split_axis=0, concat_axis=0, tiled=True)
    return arrived.astype(jnp.float32).sum(axis=0)


def sent_to_all(shard, axis):
    copies = jnp.broadcast_to(shard, (lax.axis_size(axis), *shard.shape))
    return lax.all_to_all(copies, axis, split_axis=0, concat_axis=0, tiled=True)


def joined_along(pieces, dim):
    pieces = jnp.moveaxis(pieces, 0, dim)
    dims = pieces.shape
    return pieces.reshape(*dims[:dim], dims[dim] * dims[dim + 1], *dims[dim + 2 :])


def gather_directly(shard, axis, dim):
    pieces = sent_to_all(shard, axis)
    return joined_along(pieces, dim)


def normed_rows(values, gain):
    widened = values.astype(jnp.float32)
    scale = lax.rsqrt(jnp.mean(widened * widened, axis=-1, keepdims=True) + EPSILON)
    return (widened * scale * gain).astype(jnp.bfloat16)


def later_sums(log_keep):
    cache_len = log_keep.shape[-1]
    block_len = 128
    block_count = cache_len // block_len
    lead = log_keep.shape[:-1]
    blocked = log_keep.reshape(lead + (block_count, block_len))
    rows_in = lax.broadcasted_iota(jnp.int32, (block_len, block_len), 0)
    cols_in = lax.broadcasted_iota(jnp.int32, (block_len, block_len), 1)
    upper = (rows_in >= cols_in).astype(jnp.float32)
    within = jnp.einsum("...nj,ji->...ni", blocked, upper, precision=lax.Precision.HIGHEST)
    totals = within[..., 0]
    rows_out = lax.broadcasted_iota(jnp.int32, (block_count, block_count), 0)
    cols_out = lax.broadcasted_iota(jnp.int32, (block_count, block_count), 1)
    beyond = (rows_out > cols_out).astype(jnp.float32)
    following = jnp.einsum("...m,mn->...n", totals, beyond, precision=lax.Precision.HIGHEST)
    inclusive = within + following[..., None]
    return (inclusive - blocked).reshape(log_keep.shape)


def running_ranks(present):
    count = present.shape[-1]
    rows_in = lax.broadcasted_iota(jnp.int32, (count, count), 0)
    cols_in = lax.broadcasted_iota(jnp.int32, (count, count), 1)
    lower = (rows_in <= cols_in).astype(jnp.float32)
    totals = jnp.einsum(
        "...j,ji->...i", present.astype(jnp.float32), lower, precision=lax.Precision.HIGHEST
    )
    return totals.astype(jnp.int32) - 1


def shards(
    tokens,
    norm_attn,
    w_query,
    w_key,
    w_value,
    w_out,
    attn_bias,
    cache_keys,
    cache_values,
    lengths,
    norm_ffn,
    expert_gate,
    expert_up,
    expert_down,
    dense_gate_w,
    dense_up_w,
    dense_down_w,
    dense_mix,
    routes,
    route_weights,
):
    seq_count = tokens.shape[0]
    cache_len = cache_keys.shape[1]
    group_count = cache_keys.shape[2] // HEAD_DIM
    repeat = w_query.shape[1] // (group_count * HEAD_DIM)
    normed = normed_rows(tokens, norm_attn)
    query = jnp.dot(normed, w_query, preferred_element_type=jnp.float32).astype(jnp.bfloat16)
    new_keys = jnp.dot(normed, w_key, preferred_element_type=jnp.float32).astype(jnp.bfloat16)
    new_values = jnp.dot(normed, w_value, preferred_element_type=jnp.float32).astype(jnp.bfloat16)
    query_heads = query.reshape(seq_count, group_count, repeat, HEAD_DIM)
    key_heads = cache_keys.reshape(seq_count, cache_len, group_count, HEAD_DIM)
    value_heads = cache_values.reshape(seq_count, cache_len, group_count, HEAD_DIM)
    scores = jnp.einsum(
        "bgrd,bsgd->bgrs", query_heads, key_heads, preferred_element_type=jnp.float32
    ) * HEAD_DIM ** (-0.5)
    scores = scores + attn_bias.reshape(group_count, repeat)[None, :, :, None]
    places = lax.broadcasted_iota(jnp.int32, (seq_count, cache_len), 1)
    visible = (places < lengths[:, None])[:, None, None, :]
    log_keep = jnp.where(visible, jax.nn.log_sigmoid(-scores), 0.0)
    after = later_sums(log_keep)
    weight = jnp.where(visible, jnp.exp(jax.nn.log_sigmoid(scores) + after), 0.0).astype(
        jnp.bfloat16
    )
    heads_out = jnp.einsum(
        "bgrs,bsgd->bgrd", weight, value_heads, preferred_element_type=jnp.float32
    )
    heads_out = heads_out.astype(jnp.bfloat16).reshape(seq_count, group_count * repeat * HEAD_DIM)
    partial_value = jnp.dot(heads_out, w_out, preferred_element_type=jnp.float32)
    attn_sum = sum_at_owner(partial_value.astype(jnp.bfloat16), "tp", 0)
    row_count = seq_count // lax.axis_size("tp")
    capacity = (row_count * TOP + EXPERTS - 1) // EXPERTS + 1
    own_rows = lax.dynamic_slice_in_dim(tokens, lax.axis_index("tp") * row_count, row_count, 0)
    middle = (own_rows.astype(jnp.float32) + attn_sum).astype(jnp.bfloat16)
    normed_two = normed_rows(middle, norm_ffn)
    width = normed_two.shape[1]
    piece = gather_directly(normed_two, "ep", 0)
    mix_gate = jax.nn.sigmoid(jnp.dot(piece, dense_mix, preferred_element_type=jnp.float32))
    dense_hidden = (
        jax.nn.silu(jnp.dot(piece, dense_gate_w, preferred_element_type=jnp.float32))
        * jnp.dot(piece, dense_up_w, preferred_element_type=jnp.float32)
    ).astype(jnp.bfloat16)
    dense_terms = (
        jnp.dot(dense_hidden, dense_down_w, preferred_element_type=jnp.float32) * mix_gate[:, None]
    )
    dense_term = sum_at_owner(dense_terms.astype(jnp.bfloat16), "ep", 0)
    devices = lax.axis_size(("ep", "tp"))
    members = devices // EXPERTS
    expert_ids = lax.broadcasted_iota(jnp.int32, (EXPERTS, 1, 1), 0)
    matched = routes[None, :, :] == expert_ids
    present = jnp.any(matched, axis=2).astype(jnp.int32)
    share = jnp.sum(jnp.where(matched, route_weights.astype(jnp.float32)[None, :, :], 0.0), axis=2)
    ranks = running_ranks(present)
    slot_ids = lax.broadcasted_iota(jnp.int32, (EXPERTS, capacity, row_count), 1)
    selector = (present[:, None, :] == 1) & (ranks[:, None, :] == slot_ids)
    slot_rows = jnp.einsum(
        "ecr,rk->eck", selector.astype(jnp.bfloat16), normed_two, preferred_element_type=jnp.float32
    ).astype(jnp.bfloat16)
    outgoing = jnp.repeat(slot_rows, members, axis=0)
    incoming = lax.all_to_all(outgoing, ("ep", "tp"), split_axis=0, concat_axis=0, tiled=True)
    slot_rows = incoming.reshape(devices * capacity, width)
    expert_hidden = (
        jax.nn.silu(jnp.dot(slot_rows, expert_gate, preferred_element_type=jnp.float32))
        * jnp.dot(slot_rows, expert_up, preferred_element_type=jnp.float32)
    ).astype(jnp.bfloat16)
    expert_result = jnp.dot(expert_hidden, expert_down, preferred_element_type=jnp.float32).reshape(
        devices, capacity, width
    )
    back = lax.all_to_all(
        expert_result.astype(jnp.bfloat16), ("ep", "tp"), split_axis=0, concat_axis=0, tiled=True
    ).astype(expert_result.dtype)
    per_expert = jnp.sum(back.reshape(EXPERTS, members, capacity, width), axis=1)
    expert_term = jnp.einsum("ecr,eck,er->rk", selector.astype(jnp.float32), per_expert, share)
    layer_out = (middle.astype(jnp.float32) + expert_term + dense_term).astype(jnp.bfloat16)
    return (layer_out, new_keys, new_values)


def solution(mesh):
    placed = (
        P("ep", None),
        P(),
        P(None, "tp"),
        P(None, "tp"),
        P(None, "tp"),
        P("tp", None),
        P("tp"),
        P("ep", None, "tp"),
        P("ep", None, "tp"),
        P("ep"),
        P(),
        P(None, ("ep", "tp")),
        P(None, ("ep", "tp")),
        P(("ep", "tp"), None),
        P(None, "ep"),
        P(None, "ep"),
        P("ep", None),
        P(),
        P(("ep", "tp"), None),
        P(("ep", "tp"), None),
    )
    return jax.shard_map(
        shards,
        mesh=mesh,
        in_specs=placed,
        out_specs=(P(("ep", "tp"), None), P("ep", "tp"), P("ep", "tp")),
        check_vma=False,
    )
```

profile of v0, /device:TPU:1, one launch (start us, length us, event | category | flops | bytes accessed | tf_op | source)
XLA Modules:
  0.0 196.3 jit_solution(13966771163268078858)
XLA Ops:
  1.8 2.9 %convolution_convert_fusion.4 = bf16[16,1024]{1,0:T(8,128)(2,1)S(1)} fusion(bf16[2048,1024]{1,0:T(8,128)(2,1)} %param.22, bf16[16,2048]{1,0:T(8,128)(2,1)} %param.20, f32[2048]{0:T(1024)} %param.21, f32[16]{0:T(128)S(1)} %add_rsqrt_fusion.1), kind=kOutput, calls=%fused_computation.27 | convolution fusion | flops 67256320 | bytes 4300864 | tf_op jit(solution)/shard_map/dot_general | solution.py:105
  4.8 6.4 %copy.57 = bf16[16,1024,128]{1,2,0:T(8,128)(2,1)} copy(bf16[16,1024,128]{2,1,0:T(8,128)(2,1)} %param.27) | data formatting | bytes 8388608 | tf_op args[7]
  11.4 2.8 %fusion.11 = f32[16,2,8,1024]{3,2,1,0:T(8,128)S(1)} fusion(bf16[16,2,8,64]{3,2,1,0:T(8,128)(2,1)S(1)} %reshape.91, bf16[16,1024,2,64]{1,3,2,0:T(8,128)(2,1)} %bitcast.76, f32[2,8]{1,0:T(2,128)S(1)} %add.71), kind=kOutput, calls=%fused_computation.21 | convolution fusion | flops 34078720 | bytes 5275712 | tf_op jit(solution)/shard_map/bgrd,bsgd->bgrs/dot_general | solution.py:111
  16.6 2.8 %copy.74 = f32[16,2,8,8,1]{3,2,1,0,4:T(8,128)S(1)} copy(f32[16,2,8,8,1]{4,3,2,1,0:T(8,128)} %bitcast.78) | data formatting | bytes 16384 | tf_op jit(solution)/shard_map/squeeze | solution.py:58
  19.6 2.6 %add_subtract_fusion = f32[16,2,8,8,128]{4,3,2,1,0:T(8,128)} fusion(f32[16,2,8,8,128]{4,3,2,1,0:T(8,128)} %fusion.30, f32[16,2,8,8,128]{4,2,3,1,0:T(8,128)S(1)} %fusion.27, f32[16,2,8,8]{3,2,1,0:T(8,128)S(1)} %fusion.50), kind=kLoop, calls=%fused_computation.40 | loop fusion | flops 524288 | bytes 3153920 | tf_op jit(solution)/shard_map/sub | solution.py:64
  22.2 2.4 %reshape.94 = f32[16,2,8,1024]{3,2,1,0:T(8,128)} reshape(f32[16,2,8,8,128]{4,3,2,1,0:T(8,128)} %add_subtract_fusion) | data formatting | bytes 2097152 | tf_op jit(solution)/shard_map/reshape | solution.py:64
  24.6 6.5 %copy.62 = bf16[16,1024,128]{1,2,0:T(8,128)(2,1)} copy(bf16[16,1024,128]{2,1,0:T(8,128)(2,1)} %param.28) | data formatting | bytes 8388608 | tf_op args[8]
  31.1 3.7 %convolution_convert_fusion.3 = bf16[16,2,8,64]{3,2,1,0:T(8,128)(2,1)S(1)} fusion(bf16[16,1024,2,64]{1,3,2,0:T(8,128)(2,1)} %bitcast.77, f32[16,2,8,1024]{3,2,1,0:T(8,128)} %reshape.94, f32[16,2,8,1024]{3,2,1,0:T(8,128)S(1)} %copy-done.2, pred[16,1024]{1,0:T(8,128)(4,1)S(1)} %iota_compare_fusion.1), kind=kOutput, calls=%fused_computation.26 | convolution fusion | flops 36454400 | bytes 6340608 | tf_op jit(solution)/shard_map/bgrs,bsgd->bgrd/dot_general | solution.py:122
  34.9 3.5 %fusion.1 = bf16[2,8,2048]{2,1,0:T(8,128)(2,1)} fusion(bf16[16,1024]{1,0:T(8,128)(2,1)S(1)} %reshape.96, bf16[1024,2048]{1,0:T(8,128)(2,1)} %param.25), kind=kOutput, calls=%fused_computation.9 | convolution fusion | flops 67141632 | bytes 4292608 | tf_op jit(solution)/shard_map/dot_general | solution.py:126
  38.5 4.7 %all-to-all-start = ((bf16[2,8,2048]{2,1,0:T(8,128)(2,1)}), bf16[2,8,2048]{2,1,0:T(8,128)(2,1)S(1)}, u32[]{:S(2)}, u32[]{:S(2)}) async-start(bf16[2,8,2048]{2,1,0:T(8,128)(2,1)} %fusion.1), calls=%async_computation | async-start | bytes 131072 | tf_op jit(solution)/shard_map/all_to_all | solution.py:22
  46.0 40.8 %all_to_all.25 = bf16[128,3,2048]{2,1,0:T(4,128)(2,1)} all-to-all(bf16[128,3,2048]{2,1,0:T(4,128)(2,1)S(1)} %bitcast.79), channel_id=1, replica_groups=mesh['ep'=64,'tp'=2] {'ep','tp'}, dimensions={0} | all-to-all | bytes 3145728 | tf_op jit(solution)/shard_map/all_to_all | solution.py:157
  88.3 5.7 %all-to-all-start.3 = ((bf16[64,8,2048]{2,1,0:T(8,128)(2,1)}), bf16[64,8,2048]{2,1,0:T(8,128)(2,1)}, u32[]{:S(2)}, u32[]{:S(2)}) async-start(bf16[64,8,2048]{2,1,0:T(8,128)(2,1)} %broadcast_in_dim.48), calls=%async_computation.3 | async-start | bytes 4194304 | tf_op jit(solution)/shard_map/all_to_all | solution.py:28
  94.1 3.9 %reshape.99 = bf16[384,2048]{1,0:T(8,128)(2,1)S(1)} reshape(bf16[128,3,2048]{2,1,0:T(4,128)(2,1)} %all_to_all.25) | data formatting | bytes 3145728 | tf_op jit(solution)/shard_map/reshape | solution.py:158
  98.0 3.5 %fusion.80 = f32[384,448]{0,1:T(8,128)} fusion(bf16[384,2048]{1,0:T(8,128)(2,1)S(1)} %reshape.99, bf16[2048,448]{0,1:T(8,128)(2,1)} %param.31), kind=kOutput, calls=%fused_computation.101 | convolution fusion | flops 704643072 | bytes 4096000 | tf_op jit(solution)/shard_map/dot_general | solution.py:160
  101.5 4.9 %convolution_convert_fusion = bf16[384,2048]{1,0:T(8,128)(2,1)} fusion(bf16[448,2048]{1,0:T(8,128)(2,1)S(1)} %copy-done, bf16[384,2048]{1,0:T(8,128)(2,1)S(1)} %reshape.99, bf16[2048,448]{0,1:T(8,128)(2,1)} %param.32, f32[384,448]{0,1:T(8,128)} %fusion.80), kind=kOutput, calls=%fused_computation.5 | convolution fusion | flops 1411104768 | bytes 7503872 | tf_op jit(solution)/shard_map/dot_general | solution.py:163
  106.4 5.2 %convert_element_type.104 = bf16[128,3,2048]{2,1,0:T(4,128)(2,1)} reshape(bf16[384,2048]{1,0:T(8,128)(2,1)} %convolution_convert_fusion) | data formatting | bytes 3145728 | tf_op jit(solution)/shard_map/convert_element_type | solution.py:167
  111.6 10.7 %all-to-all-done.3 = bf16[64,8,2048]{2,1,0:T(8,128)(2,1)} async-done(((bf16[64,8,2048]{2,1,0:T(8,128)(2,1)}), bf16[64,8,2048]{2,1,0:T(8,128)(2,1)}, u32[]{:S(2)}, u32[]{:S(2)}) %all-to-all-start.3) | async-done | bytes 2097184 | tf_op jit(solution)/shard_map/all_to_all | solution.py:28
  122.2 7.3 %all-to-all-start.2 = ((bf16[128,3,2048]{2,1,0:T(4,128)(2,1)}), bf16[128,3,2048]{2,1,0:T(4,128)(2,1)}, u32[]{:S(2)}, u32[]{:S(2)}) async-start(bf16[128,3,2048]{2,1,0:T(4,128)(2,1)} %convert_element_type.104), calls=%async_computation.2 | async-start | bytes 4194304 | tf_op jit(solution)/shard_map/all_to_all | solution.py:166
  132.0 2.4 %fusion.9 = f32[512,112]{0,1:T(8,128)S(1)} fusion(bf16[2048,112]{0,1:T(8,128)(2,1)S(1)} %copy-done.8, bf16[64,8,2048]{2,1,0:T(8,128)(2,1)} %all-to-all-done.3), kind=kOutput, calls=%fused_computation.18 | convolution fusion | flops 234881024 | bytes 2785280 | tf_op jit(solution)/shard_map/dot_general | solution.py:137
  134.4 4.5 %fusion = bf16[64,8,2048]{2,1,0:T(8,128)(2,1)} fusion(bf16[112,2048]{1,0:T(8,128)(2,1)S(1)} %copy-done.6, f32[512]{0:T(512)S(1)} %add_divide_fusion, bf16[2048,112]{0,1:T(8,128)(2,1)S(1)} %copy-done.7, bf16[64,8,2048]{2,1,0:T(8,128)(2,1)} %all-to-all-done.3, f32[512,112]{0,1:T(8,128)S(1)} %fusion.9), kind=kOutput, calls=%fused_computation.6 | convolution fusion | flops 472203264 | bytes 5343232 | tf_op jit(solution)/shard_map/dot_general | solution.py:141
  138.9 20.8 %all-to-all-done.2 = bf16[128,3,2048]{2,1,0:T(4,128)(2,1)} async-done(((bf16[128,3,2048]{2,1,0:T(4,128)(2,1)}), bf16[128,3,2048]{2,1,0:T(4,128)(2,1)}, u32[]{:S(2)}, u32[]{:S(2)}) %all-to-all-start.2) | async-done | bytes 1572896 | tf_op jit(solution)/shard_map/all_to_all | solution.py:166
  159.7 5.6 %all-to-all-start.4 = ((bf16[64,8,2048]{2,1,0:T(8,128)(2,1)}), bf16[64,8,2048]{2,1,0:T(8,128)(2,1)}, u32[]{:S(2)}, u32[]{:S(2)}) async-start(bf16[64,8,2048]{2,1,0:T(8,128)(2,1)} %fusion), calls=%async_computation.4 | async-start | bytes 4194304 | tf_op jit(solution)/shard_map/all_to_all | solution.py:22
  167.0 2.7 %convert_reduce_fusion = bf16[8,3,2048]{2,1,0:T(4,128)(2,1)S(1)} fusion(bf16[128,3,2048]{2,1,0:T(4,128)(2,1)} %all-to-all-done.2), kind=kLoop, calls=%fused_computation | loop fusion | flops 1523712 | bytes 1671168 | tf_op jit(solution)/shard_map/reduce_sum | solution.py:169
  169.7 23.8 %all-to-all-done.4 = bf16[64,8,2048]{2,1,0:T(8,128)(2,1)} async-done(((bf16[64,8,2048]{2,1,0:T(8,128)(2,1)}), bf16[64,8,2048]{2,1,0:T(8,128)(2,1)}, u32[]{:S(2)}, u32[]{:S(2)}) %all-to-all-start.4) | async-done | bytes 2097184 | tf_op jit(solution)/shard_map/all_to_all | solution.py:22
  (65 shorter events, 15.3 us)
Async XLA Ops:
  0.6 100.9 %copy-start = (bf16[448,2048]{1,0:T(8,128)(2,1)S(1)}, bf16[448,2048]{1,0:T(8,128)(2,1)}, u32[]{:S(2)}) copy-start(bf16[448,2048]{1,0:T(8,128)(2,1)} %param.33) | copy-start | bytes 5505028
  4.8 6.4 %copy-start.14 = (f32[16]{0:T(128)S(1)}, f32[16]{0:T(128)}, u32[]{:S(2)}) copy-start(f32[16]{0:T(128)} %param.26) | copy-start | bytes 196
  4.8 6.5 %copy-start.13 = (s32[16]{0:T(128)S(1)}, s32[16]{0:T(128)}, u32[]{:S(2)}) copy-start(s32[16]{0:T(128)} %param.29) | copy-start | bytes 196
  14.3 2.3 %copy-start.1 = (f32[16,2,8,1024]{3,2,1,0:T(8,128)}, f32[16,2,8,1024]{3,2,1,0:T(8,128)S(1)}, u32[]{:S(2)}) copy-start(f32[16,2,8,1024]{3,2,1,0:T(8,128)S(1)} %fusion.11) | copy-start | bytes 3145732
  24.6 6.5 %copy-start.2 = (f32[16,2,8,1024]{3,2,1,0:T(8,128)S(1)}, f32[16,2,8,1024]{3,2,1,0:T(8,128)}, u32[]{:S(2)}) copy-start(f32[16,2,8,1024]{3,2,1,0:T(8,128)} %copy-done.1) | copy-start | bytes 3145732
  34.9 8.2 %copy-start.12 = (s32[8,2]{0,1:T(2,128)S(1)}, s32[8,2]{0,1:T(2,128)}, u32[]{:S(2)}) copy-start(s32[8,2]{0,1:T(2,128)} %param.38) | copy-start | bytes 196
  34.9 9.3 %copy-start.3 = (bf16[16,2048]{1,0:T(8,128)(2,1)S(1)}, bf16[16,2048]{1,0:T(8,128)(2,1)}, u32[]{:S(2)}) copy-start(bf16[16,2048]{1,0:T(8,128)(2,1)} %param.20) | copy-start | bytes 196612
  34.9 9.6 %copy-start.10 = (f32[2048]{0:T(1024)S(1)}, f32[2048]{0:T(1024)}, u32[]{:S(2)}) copy-start(f32[2048]{0:T(1024)} %param.30) | copy-start | bytes 24580
  38.5 5.7 %all-to-all-start = ((bf16[2,8,2048]{2,1,0:T(8,128)(2,1)}), bf16[2,8,2048]{2,1,0:T(8,128)(2,1)S(1)}, u32[]{:S(2)}, u32[]{:S(2)}) async-start(bf16[2,8,2048]{2,1,0:T(8,128)(2,1)} %fusion.1), calls=%async_computation | async-start | bytes 131072 | tf_op jit(solution)/shard_map/all_to_all | solution.py:22
  88.3 33.9 %all-to-all-start.3 = ((bf16[64,8,2048]{2,1,0:T(8,128)(2,1)}), bf16[64,8,2048]{2,1,0:T(8,128)(2,1)}, u32[]{:S(2)}, u32[]{:S(2)}) async-start(bf16[64,8,2048]{2,1,0:T(8,128)(2,1)} %broadcast_in_dim.48), calls=%async_computation.3 | async-start | bytes 4194304 | tf_op jit(solution)/shard_map/all_to_all | solution.py:28
  111.6 18.0 %copy-start.11 = (bf16[2048]{0:T(1024)(128)(2,1)S(1)}, bf16[2048]{0:T(1024)(128)(2,1)}, u32[]{:S(2)}) copy-start(bf16[2048]{0:T(1024)(128)(2,1)} %param.37) | copy-start | bytes 12292
  122.2 37.4 %all-to-all-start.2 = ((bf16[128,3,2048]{2,1,0:T(4,128)(2,1)}), bf16[128,3,2048]{2,1,0:T(4,128)(2,1)}, u32[]{:S(2)}, u32[]{:S(2)}) async-start(bf16[128,3,2048]{2,1,0:T(4,128)(2,1)} %convert_element_type.104), calls=%async_computation.2 | async-start | bytes 4194304 | tf_op jit(solution)/shard_map/all_to_all | solution.py:166
  129.6 2.4 %copy-start.8 = (bf16[2048,112]{0,1:T(8,128)(2,1)S(1)}, bf16[2048,112]{0,1:T(8,128)(2,1)}, u32[]{:S(2)}) copy-start(bf16[2048,112]{0,1:T(8,128)(2,1)} %param.34) | copy-start | bytes 1376260
  129.6 4.8 %copy-start.6 = (bf16[112,2048]{1,0:T(8,128)(2,1)S(1)}, bf16[112,2048]{1,0:T(8,128)(2,1)}, u32[]{:S(2)}) copy-start(bf16[112,2048]{1,0:T(8,128)(2,1)} %param.36) | copy-start | bytes 1376260
  129.6 4.8 %copy-start.7 = (bf16[2048,112]{0,1:T(8,128)(2,1)S(1)}, bf16[2048,112]{0,1:T(8,128)(2,1)}, u32[]{:S(2)}) copy-start(bf16[2048,112]{0,1:T(8,128)(2,1)} %param.35) | copy-start | bytes 1376260
  138.9 26.4 %copy-start.15 = (bf16[8,2]{0,1:T(2,128)(2,1)S(1)}, bf16[8,2]{0,1:T(2,128)(2,1)}, u32[]{:S(2)}) copy-start(bf16[8,2]{0,1:T(2,128)(2,1)} %param.39) | copy-start | bytes 100
  138.9 26.5 %copy-start.4 = (bf16[2048,128]{1,0:T(8,128)(2,1)S(1)}, bf16[2048,128]{1,0:T(8,128)(2,1)}, u32[]{:S(2)}) copy-start(bf16[2048,128]{1,0:T(8,128)(2,1)} %param.24) | copy-start | bytes 1572868
  138.9 26.5 %copy-start.9 = (f32[2048]{0:T(1024)S(1)}, f32[2048]{0:T(1024)}, u32[]{:S(2)}) copy-start(f32[2048]{0:T(1024)} %param.21) | copy-start | bytes 24580
  138.9 27.3 %copy-start.5 = (bf16[2048,128]{1,0:T(8,128)(2,1)S(1)}, bf16[2048,128]{1,0:T(8,128)(2,1)}, u32[]{:S(2)}) copy-start(bf16[2048,128]{1,0:T(8,128)(2,1)} %param.23) | copy-start | bytes 1572868
  159.7 33.9 %all-to-all-start.4 = ((bf16[64,8,2048]{2,1,0:T(8,128)(2,1)}), bf16[64,8,2048]{2,1,0:T(8,128)(2,1)}, u32[]{:S(2)}, u32[]{:S(2)}) async-start(bf16[64,8,2048]{2,1,0:T(8,128)(2,1)} %fusion), calls=%async_computation.4 | async-start | bytes 4194304 | tf_op jit(solution)/shard_map/all_to_all | solution.py:22
where the time goes:
time: 199 us; the launch traced here: 196 us
  waiting for transfers between devices  56.2 us (28%)
  blocking collectives  40.8 us (21%)
  matrix products  35.3 us (18%)
  local copies, waits for them, and re-layouts  30.4 us (15%)
  starting transfers between devices  23.3 us (12%)
  other arithmetic  9.33 us (5%)
    all_to_all x1, blocking collectives, shards(): lax.all_to_all(outgoing, ('ep', 'tp'), split_axis=0, concat_axis=0, tiled...  40.8 us
    all_to_all x2, waiting for transfers between devices, sum_at_owner(): lax.all_to_all(pieces, axis, split_axis=0, concat_axis=0, tiled=True)  24.7 us
    all_to_all x1, waiting for transfers between devices, shards(): lax.all_to_all(expert_result.astype(jnp.bfloat16), ('ep', 'tp'), split_ax...  20.8 us
    unnamed x35, local copies, waits for them, and re-layouts  13 us
    all_to_all x1, waiting for transfers between devices, sent_to_all(): return lax.all_to_all(copies, axis, split_axis=0, concat_axis=0, tiled=True)  10.7 us
    all_to_all x2, starting transfers between devices, sum_at_owner(): lax.all_to_all(pieces, axis, split_axis=0, concat_axis=0, tiled=True)  10.2 us
    all_to_all x1, starting transfers between devices, shards(): lax.all_to_all(expert_result.astype(jnp.bfloat16), ('ep', 'tp'), split_ax...  7.32 us
    all_to_all x1, starting transfers between devices, sent_to_all(): return lax.all_to_all(copies, axis, split_axis=0, concat_axis=0, tiled=True)  5.74 us
  transfers between devices with their start and end apart: 4, of which 4 were waited for; matrix products, arithmetic and copies ran while one was open for 16% of the time, Pallas kernels for 0%

commit v1 on v0

--- a/solution.py
+++ b/solution.py
@@ -1,14 +1,162 @@
+import functools
 import jax
 import jax.numpy as jnp
 from jax import lax
+from jax.experimental import pallas as pl
+from jax.experimental.pallas import tpu as pltpu
 from jax.sharding import PartitionSpec as P
 
-HEAD_DIM = 64
+D = 2048
+BF = jnp.bfloat16
+F32 = jnp.float32
+EPSILON = 1e-06
+SEQS = 16
+CACHE = 1024
+HEADS = 16
+NT = (((1,), (1,)), ((), ()))
+VM = pl.BlockSpec(memory_space=pltpu.VMEM)
+HB = pl.BlockSpec(memory_space=pl.ANY)
+
+
+def normed_rows(widened, gain):
+    scale = lax.rsqrt(jnp.mean(widened * widened, axis=-1, keepdims=True) + EPSILON)
+    return (widened * scale * gain).astype(BF)
+
+
+def column_of(row, count):
+    rows = lax.broadcasted_iota(jnp.int32, (count, count), 0)
+    cols = lax.broadcasted_iota(jnp.int32, (count, count), 1)
+    wide = jnp.broadcast_to(row, (count, count))
+    return jnp.sum(jnp.where(rows == cols, wide, 0.0), axis=1, keepdims=True)
+
+
+def attention_kernel(
+    tokens, norm, bias, lengths, wq_h, wk_h, wv_h, wo_h, ck_h, cv_h,
+    part, nk, nv,
+    wq, wk, wv, wo, ck, cv, qs, xs, sq, sw, so, sk, sv,
+):
+    def q_copy(i):
+        rows = pl.ds(i * 512, 512)
+        return pltpu.make_async_copy(wq_h.at[rows], wq.at[rows], sq.at[i])
+
+    def o_copy(i):
+        place = (i % 8) * 128 + (i // 8) * 64
+        return pltpu.make_async_copy(wo_h.at[pl.ds(i * 64, 64)], wo.at[pl.ds(place, 64)], so.at[i])
+
+    def k_copy(b):
+        return pltpu.make_async_copy(ck_h.at[b], ck.at[b], sk.at[b])
+
+    def v_copy(b):
+        return pltpu.make_async_copy(cv_h.at[b], cv.at[b], sv.at[b])
+
+    wk_copy = pltpu.make_async_copy(wk_h, wk, sw.at[0])
+    wv_copy = pltpu.make_async_copy(wv_h, wv, sw.at[1])
+    for i in range(4):
+        q_copy(i).start()
+    for b in range(SEQS):
+        k_copy(b).start()
+        v_copy(b).start()
+    for i in range(16):
+        o_copy(i).start()
+    wk_copy.start()
+    wv_copy.start()
+
+    normed = normed_rows(tokens[...].astype(F32), norm[...])
+    query = jnp.zeros((SEQS, HEADS * 64), F32)
+    for i in range(4):
+        q_copy(i).wait()
+        query += jnp.dot(normed[:, i * 512 : (i + 1) * 512], wq[pl.ds(i * 512, 512), :], preferred_element_type=F32)
+    query = query.astype(BF).astype(F32) * 0.125
+    lane = lax.broadcasted_iota(jnp.int32, (SEQS, 128), 1)
+    for i in range(8):
+        pair = query[:, i * 128 : (i + 1) * 128]
+        turned = pltpu.roll(pair, 64, 1)
+        for j in range(2):
+            h = 2 * i + j
+            low = h < 8
+            chosen = pair if (j == 0) == low else turned
+            keep = (lane < 64) if low else (lane >= 64)
+            qs[:, h, :] = jnp.where(keep, chosen, 0.0)
+
+    bias_col = column_of(bias[...], HEADS)
+    tri = (
+        lax.broadcasted_iota(jnp.int32, (256, 256), 0) > lax.broadcasted_iota(jnp.int32, (256, 256), 1)
+    ).astype(BF)
+    places = lax.broadcasted_iota(jnp.int32, (HEADS, CACHE), 1)
+    lane8 = lax.broadcasted_iota(jnp.int32, (8, 128), 1)
+
+    def one_sequence(b):
+        k_copy(b).wait()
+        z = lax.dot_general(qs[b].astype(BF), ck[b], NT, preferred_element_type=F32) + bias_col
+        visible = places < lengths[b]
+        tail = jnp.log(1.0 + jnp.exp(-jnp.abs(z)))
+        log_take = jnp.minimum(z, 0.0) - tail
+        log_keep = jnp.where(visible, jnp.minimum(-z, 0.0) - tail, 0.0)
+        high = log_keep.astype(BF)
+        rest = (log_keep - high.astype(F32)).astype(BF)
+        blocks = [high[:, n * 256 : (n + 1) * 256] for n in range(4)]
+        blocks += [rest[:, n * 256 : (n + 1) * 256] for n in range(4)]
+        sums = jnp.dot(jnp.concatenate(blocks, axis=0), tri, preferred_element_type=F32)
+        later = jnp.zeros((HEADS, 1), F32)
+        after = [None] * 4
+        for n in range(3, -1, -1):
+            inner = sums[n * 16 : (n + 1) * 16] + sums[64 + n * 16 : 64 + (n + 1) * 16]
+            after[n] = inner + later
+            later = later + inner[:, 0:1] + log_keep[:, n * 256 : n * 256 + 1]
+        weight = jnp.where(visible, jnp.exp(log_take + jnp.concatenate(after, axis=1)), 0.0).astype(BF)
+        v_copy(b).wait()
+        mixed = jnp.dot(weight, cv[b], preferred_element_type=F32)
+        xs[b] = jnp.where(lane8 < 64, mixed[0:8], mixed[8:16])
+
+    def some(i, carry):
+        for j in range(4):
+            one_sequence(i * 4 + j)
+        return carry
+
+    lax.fori_loop(0, SEQS // 4, some, 0)
+
+    for i in range(16):
+        o_copy(i).wait()
+    heads = jnp.concatenate([xs[:, r, :].astype(BF) for r in range(8)], axis=1)
+    part[...] = jnp.dot(heads, wo[...], preferred_element_type=F32).astype(BF)
+    wk_copy.wait()
+    wv_copy.wait()
+    nk[...] = jnp.dot(normed, wk[...], preferred_element_type=F32).astype(BF)
+    nv[...] = jnp.dot(normed, wv[...], preferred_element_type=F32).astype(BF)
+
+
+def attention(tokens, norm, bias, lengths, wq, wk, wv, wo, ck, cv):
+    return pl.pallas_call(
+        attention_kernel,
+        out_shape=(
+            jax.ShapeDtypeStruct((SEQS, D), BF),
+            jax.ShapeDtypeStruct((SEQS, 128), BF),
+            jax.ShapeDtypeStruct((SEQS, 128), BF),
+        ),
+        in_specs=[VM, VM, VM, pl.BlockSpec(memory_space=pltpu.SMEM)] + [HB] * 6,
+        out_specs=(VM, VM, VM),
+        scratch_shapes=[
+            pltpu.VMEM((D, 1024), BF),
+            pltpu.VMEM((D, 128), BF),
+            pltpu.VMEM((D, 128), BF),
+            pltpu.VMEM((1024, D), BF),
+            pltpu.VMEM((SEQS, CACHE, 128), BF),
+            pltpu.VMEM((SEQS, CACHE, 128), BF),
+            pltpu.VMEM((SEQS, HEADS, 128), F32),
+            pltpu.VMEM((SEQS, 8, 128), F32),
+            pltpu.SemaphoreType.DMA((4,)),
+            pltpu.SemaphoreType.DMA((2,)),
+            pltpu.SemaphoreType.DMA((16,)),
+            pltpu.SemaphoreType.DMA((SEQS,)),
+            pltpu.SemaphoreType.DMA((SEQS,)),
+        ],
+        compiler_params=pltpu.CompilerParams(vmem_limit_bytes=40 * 1024 * 1024),
+        name="attention",
+    )(tokens, norm.reshape(1, D), bias.reshape(1, HEADS), lengths, wq, wk, wv, wo, ck, cv)
+
+
 EXPERTS = 8
 TOP = 2
-
-
-EPSILON = 1e-06
 
 
 def split_up(shard, dim, count):
@@ -37,31 +185,6 @@
 def gather_directly(shard, axis, dim):
     pieces = sent_to_all(shard, axis)
     return joined_along(pieces, dim)
-
-
-def normed_rows(values, gain):
-    widened = values.astype(jnp.float32)
-    scale = lax.rsqrt(jnp.mean(widened * widened, axis=-1, keepdims=True) + EPSILON)
-    return (widened * scale * gain).astype(jnp.bfloat16)
-
-
-def later_sums(log_keep):
-    cache_len = log_keep.shape[-1]
-    block_len = 128
-    block_count = cache_len // block_len
-    lead = log_keep.shape[:-1]
-    blocked = log_keep.reshape(lead + (block_count, block_len))
-    rows_in = lax.broadcasted_iota(jnp.int32, (block_len, block_len), 0)
-    cols_in = lax.broadcasted_iota(jnp.int32, (block_len, block_len), 1)
-    upper = (rows_in >= cols_in).astype(jnp.float32)
-    within = jnp.einsum("...nj,ji->...ni", blocked, upper, precision=lax.Precision.HIGHEST)
-    totals = within[..., 0]
-    rows_out = lax.broadcasted_iota(jnp.int32, (block_count, block_count), 0)
-    cols_out = lax.broadcasted_iota(jnp.int32, (block_count, block_count), 1)
-    beyond = (rows_out > cols_out).astype(jnp.float32)
-    following = jnp.einsum("...m,mn->...n", totals, beyond, precision=lax.Precision.HIGHEST)
-    inclusive = within + following[..., None]
-    return (inclusive - blocked).reshape(log_keep.shape)
 
 
 def running_ranks(present):
@@ -98,38 +221,15 @@
     route_weights,
 ):
     seq_count = tokens.shape[0]
-    cache_len = cache_keys.shape[1]
-    group_count = cache_keys.shape[2] // HEAD_DIM
-    repeat = w_query.shape[1] // (group_count * HEAD_DIM)
-    normed = normed_rows(tokens, norm_attn)
-    query = jnp.dot(normed, w_query, preferred_element_type=jnp.float32).astype(jnp.bfloat16)
-    new_keys = jnp.dot(normed, w_key, preferred_element_type=jnp.float32).astype(jnp.bfloat16)
-    new_values = jnp.dot(normed, w_value, preferred_element_type=jnp.float32).astype(jnp.bfloat16)
-    query_heads = query.reshape(seq_count, group_count, repeat, HEAD_DIM)
-    key_heads = cache_keys.reshape(seq_count, cache_len, group_count, HEAD_DIM)
-    value_heads = cache_values.reshape(seq_count, cache_len, group_count, HEAD_DIM)
-    scores = jnp.einsum(
-        "bgrd,bsgd->bgrs", query_heads, key_heads, preferred_element_type=jnp.float32
-    ) * HEAD_DIM ** (-0.5)
-    scores = scores + attn_bias.reshape(group_count, repeat)[None, :, :, None]
-    places = lax.broadcasted_iota(jnp.int32, (seq_count, cache_len), 1)
-    visible = (places < lengths[:, None])[:, None, None, :]
-    log_keep = jnp.where(visible, jax.nn.log_sigmoid(-scores), 0.0)
-    after = later_sums(log_keep)
-    weight = jnp.where(visible, jnp.exp(jax.nn.log_sigmoid(scores) + after), 0.0).astype(
-        jnp.bfloat16
-    )
-    heads_out = jnp.einsum(
-        "bgrs,bsgd->bgrd", weight, value_heads, preferred_element_type=jnp.float32
-    )
-    heads_out = heads_out.astype(jnp.bfloat16).reshape(seq_count, group_count * repeat * HEAD_DIM)
-    partial_value = jnp.dot(heads_out, w_out, preferred_element_type=jnp.float32)
-    attn_sum = sum_at_owner(partial_value.astype(jnp.bfloat16), "tp", 0)
+    partial_value, new_keys, new_values = attention(
+        tokens, norm_attn, attn_bias, lengths, w_query, w_key, w_value, w_out, cache_keys, cache_values
+    )
+    attn_sum = sum_at_owner(partial_value, "tp", 0)
     row_count = seq_count // lax.axis_size("tp")
     capacity = (row_count * TOP + EXPERTS - 1) // EXPERTS + 1
     own_rows = lax.dynamic_slice_in_dim(tokens, lax.axis_index("tp") * row_count, row_count, 0)
     middle = (own_rows.astype(jnp.float32) + attn_sum).astype(jnp.bfloat16)
-    normed_two = normed_rows(middle, norm_ffn)
+    normed_two = normed_rows(middle.astype(F32), norm_ffn)
     width = normed_two.shape[1]
     piece = gather_directly(normed_two, "ep", 0)
     mix_gate = jax.nn.sigmoid(jnp.dot(piece, dense_mix, preferred_element_type=jnp.float32))

time: 199 us -> 186 us (0.935)
  matrix products: 35.3 us -> 18.8 us
  Pallas kernels: 0 us -> 14.1 us
  local copies, waits for them, and re-layouts: 30.4 us -> 23.7 us
  other arithmetic: 9.33 us -> 4.87 us
    dot_general x8 -> x0, matrix products: 16.6 us -> none  [the longest x1 3.72 us: shards(): jnp.einsum('bgrs,bsgd->bgrd', weight, value_heads, preferred_element_type...]
    pallas_call x0 -> x1, Pallas kernels: none -> 14.1 us  [attention(): pl.pallas_call(attention_kernel, out_shape=(jax.ShapeDtypeStruct((SEQS, D...]
    squeeze x1 -> x0, local copies, waits for them, and re-layouts: 2.76 us -> none  [later_sums(): totals = within[..., 0]]
    reshape x3 -> x0, local copies, waits for them, and re-layouts: 2.63 us -> none  [the longest x1 2.39 us: later_sums(): return (inclusive - blocked).reshape(log_keep.shape)]
    sub x1 -> x0, other arithmetic: 2.6 us -> none  [later_sums(): return (inclusive - blocked).reshape(log_keep.shape)]
    unnamed x35 -> x37, local copies, waits for them, and re-layouts: 13 us -> 11.7 us
where the time goes in v1:
time: 186 us; the launch traced here: 184 us
  waiting for transfers between devices  58 us (31%)
  blocking collectives  40.8 us (22%)
  local copies, waits for them, and re-layouts  23.7 us (13%)
  starting transfers between devices  23.2 us (12%)
  matrix products  18.8 us (10%)
  Pallas kernels  14.1 us (8%)
  other arithmetic  4.87 us (3%)
    all_to_all x1, blocking collectives, shards(): lax.all_to_all(outgoing, ('ep', 'tp'), split_axis=0, concat_axis=0, tiled...  40.8 us
    all_to_all x2, waiting for transfers between devices, sum_at_owner(): lax.all_to_all(pieces, axis, split_axis=0, concat_axis=0, tiled=True)  26.4 us
    all_to_all x1, waiting for transfers between devices, shards(): lax.all_to_all(expert_result.astype(jnp.bfloat16), ('ep', 'tp'), split_ax...  20.8 us
    pallas_call x1, Pallas kernels, attention(): pl.pallas_call(attention_kernel, out_shape=(jax.ShapeDtypeStruct((SEQS, D...  14.1 us
    unnamed x37, local copies, waits for them, and re-layouts  11.7 us
    all_to_all x1, waiting for transfers between devices, sent_to_all(): return lax.all_to_all(copies, axis, split_axis=0, concat_axis=0, tiled=True)  10.8 us
    all_to_all x2, starting transfers between devices, sum_at_owner(): lax.all_to_all(pieces, axis, split_axis=0, concat_axis=0, tiled=True)  10.3 us
    all_to_all x1, starting transfers between devices, shards(): lax.all_to_all(expert_result.astype(jnp.bfloat16), ('ep', 'tp'), split_ax...  7.34 us
  transfers between devices with their start and end apart: 4, of which 4 were waited for; matrix products, arithmetic and copies ran while one was open for 16% of the time, Pallas kernels for 0%

profile of v1, /device:TPU:1, one launch (start us, length us, event | category | flops | bytes accessed | tf_op | source)
XLA Modules:
  0.0 184.2 jit_solution(3617538241391784777)
XLA Ops:
  0.7 2.3 %copy-done.1 = bf16[2048,1024]{1,0:T(8,128)(2,1)S(1)} copy-done((bf16[2048,1024]{1,0:T(8,128)(2,1)S(1)}, bf16[2048,1024]{1,0:T(8,128)(2,1)}, u32[]{:S(2)}) %copy-start.1) | copy-done | bytes 4194328
  3.0 2.2 %copy-done.2 = bf16[1024,2048]{1,0:T(8,128)(2,1)S(1)} copy-done((bf16[1024,2048]{1,0:T(8,128)(2,1)S(1)}, bf16[1024,2048]{1,0:T(8,128)(2,1)}, u32[]{:S(2)}) %copy-start.2) | copy-done | bytes 4194328
  5.2 2.2 %copy-done.3 = bf16[16,1024,128]{2,1,0:T(8,128)(2,1)S(1)} copy-done((bf16[16,1024,128]{2,1,0:T(8,128)(2,1)S(1)}, bf16[16,1024,128]{2,1,0:T(8,128)(2,1)}, u32[]{:S(2)}) %copy-start.3) | copy-done | bytes 4194328
  7.4 1.0 copy-done.4
  8.4 1.0 copy-done.5
  12.3 14.1 %attention.1 = (bf16[16,2048]{1,0:T(8,128)(2,1)}, bf16[16,128]{1,0:T(8,128)(2,1)}, bf16[16,128]{1,0:T(8,128)(2,1)}) custom-call(bf16[16,2048]{1,0:T(8,128)(2,1)S(1)} %copy-done.6, f32[1,2048]{1,0:T(1,128)S(1)} %bitcast.46, f32[1,16]{1,0:T(1,128)S(1)} %bitcast.47, s32[16]{0:T(128)S(1)} %copy-done.10, bf16[2048,1024]{1,0:T(8,128)(2,1)S(1)} %copy-done.1, ...), custom_call_target="tpu_custom_call" | custom-call | tf_op jit(solution)/shard_map/attention/pallas_call | solution.py:129
  26.4 4.7 %all-to-all-start = ((bf16[2,8,2048]{2,1,0:T(8,128)(2,1)}), bf16[2,8,2048]{2,1,0:T(8,128)(2,1)S(1)}, u32[]{:S(2)}, u32[]{:S(2)}) async-start(bf16[2,8,2048]{2,1,0:T(8,128)(2,1)} %bitcast.2), calls=%async_computation | async-start | bytes 131072 | tf_op jit(solution)/shard_map/all_to_all | solution.py:170
  33.9 40.8 %all_to_all.25 = bf16[128,3,2048]{2,1,0:T(4,128)(2,1)} all-to-all(bf16[128,3,2048]{2,1,0:T(4,128)(2,1)S(1)} %bitcast.48), channel_id=1, replica_groups=mesh['ep'=64,'tp'=2] {'ep','tp'}, dimensions={0} | all-to-all | bytes 3145728 | tf_op jit(solution)/shard_map/all_to_all | solution.py:257
  74.7 1.6 broadcast_in_dim.28
  76.3 5.6 %all-to-all-start.3 = ((bf16[64,8,2048]{2,1,0:T(8,128)(2,1)}), bf16[64,8,2048]{2,1,0:T(8,128)(2,1)}, u32[]{:S(2)}, u32[]{:S(2)}) async-start(bf16[64,8,2048]{2,1,0:T(8,128)(2,1)} %broadcast_in_dim.28), calls=%async_computation.3 | async-start | bytes 4194304 | tf_op jit(solution)/shard_map/all_to_all | solution.py:176
  81.9 3.9 %reshape.57 = bf16[384,2048]{1,0:T(8,128)(2,1)S(1)} reshape(bf16[128,3,2048]{2,1,0:T(4,128)(2,1)} %all_to_all.25) | data formatting | bytes 3145728 | tf_op jit(solution)/shard_map/reshape | solution.py:258
  85.8 3.5 %fusion.52 = f32[384,448]{0,1:T(8,128)} fusion(bf16[384,2048]{1,0:T(8,128)(2,1)S(1)} %reshape.57, bf16[2048,448]{0,1:T(8,128)(2,1)} %param.31), kind=kOutput, calls=%fused_computation.64 | convolution fusion | flops 704643072 | bytes 4096000 | tf_op jit(solution)/shard_map/dot_general | solution.py:260
  89.3 4.9 %convolution_convert_fusion = bf16[384,2048]{1,0:T(8,128)(2,1)} fusion(bf16[448,2048]{1,0:T(8,128)(2,1)S(1)} %copy-done, bf16[384,2048]{1,0:T(8,128)(2,1)S(1)} %reshape.57, bf16[2048,448]{0,1:T(8,128)(2,1)} %param.32, f32[384,448]{0,1:T(8,128)} %fusion.52), kind=kOutput, calls=%fused_computation.3 | convolution fusion | flops 1411104768 | bytes 7503872 | tf_op jit(solution)/shard_map/dot_general | solution.py:263
  94.2 5.2 %convert_element_type.72 = bf16[128,3,2048]{2,1,0:T(4,128)(2,1)} reshape(bf16[384,2048]{1,0:T(8,128)(2,1)} %convolution_convert_fusion) | data formatting | bytes 3145728 | tf_op jit(solution)/shard_map/convert_element_type | solution.py:267
  99.4 10.8 %all-to-all-done.3 = bf16[64,8,2048]{2,1,0:T(8,128)(2,1)} async-done(((bf16[64,8,2048]{2,1,0:T(8,128)(2,1)}), bf16[64,8,2048]{2,1,0:T(8,128)(2,1)}, u32[]{:S(2)}, u32[]{:S(2)}) %all-to-all-start.3) | async-done | bytes 2097184 | tf_op jit(solution)/shard_map/all_to_all | solution.py:176
  110.2 7.3 %all-to-all-start.2 = ((bf16[128,3,2048]{2,1,0:T(4,128)(2,1)}), bf16[128,3,2048]{2,1,0:T(4,128)(2,1)}, u32[]{:S(2)}, u32[]{:S(2)}) async-start(bf16[128,3,2048]{2,1,0:T(4,128)(2,1)} %convert_element_type.72), calls=%async_computation.2 | async-start | bytes 4194304 | tf_op jit(solution)/shard_map/all_to_all | solution.py:266
  117.6 2.3 %fusion.4 = f32[1,512]{1,0:T(1,128)S(1)} fusion(bf16[2048,1]{0,1:T(2,128)(2,1)S(1)} %reshape.66, bf16[64,8,2048]{2,1,0:T(8,128)(2,1)} %all-to-all-done.3), kind=kOutput, calls=%fused_computation.10 | convolution fusion | flops 2097152 | bytes 2103296 | tf_op jit(solution)/shard_map/dot_general | solution.py:235
  119.9 2.4 %fusion.8 = f32[512,112]{0,1:T(8,128)S(1)} fusion(bf16[2048,112]{0,1:T(8,128)(2,1)S(1)} %copy-done.13, bf16[64,8,2048]{2,1,0:T(8,128)(2,1)} %all-to-all-done.3), kind=kOutput, calls=%fused_computation.14 | convolution fusion | flops 234881024 | bytes 2785280 | tf_op jit(solution)/shard_map/dot_general | solution.py:237
  122.4 4.5 %fusion = bf16[64,8,2048]{2,1,0:T(8,128)(2,1)} fusion(bf16[112,2048]{1,0:T(8,128)(2,1)S(1)} %copy-done.11, f32[512]{0:T(512)S(1)} %add_divide_fusion, bf16[2048,112]{0,1:T(8,128)(2,1)S(1)} %copy-done.12, bf16[64,8,2048]{2,1,0:T(8,128)(2,1)} %all-to-all-done.3, f32[512,112]{0,1:T(8,128)S(1)} %fusion.8), kind=kOutput, calls=%fused_computation.4 | convolution fusion | flops 472203264 | bytes 5343232 | tf_op jit(solution)/shard_map/dot_general | solution.py:241
  126.9 20.8 %all-to-all-done.2 = bf16[128,3,2048]{2,1,0:T(4,128)(2,1)} async-done(((bf16[128,3,2048]{2,1,0:T(4,128)(2,1)}), bf16[128,3,2048]{2,1,0:T(4,128)(2,1)}, u32[]{:S(2)}, u32[]{:S(2)}) %all-to-all-start.2) | async-done | bytes 1572896 | tf_op jit(solution)/shard_map/all_to_all | solution.py:266
  147.6 5.6 %all-to-all-start.4 = ((bf16[64,8,2048]{2,1,0:T(8,128)(2,1)}), bf16[64,8,2048]{2,1,0:T(8,128)(2,1)}, u32[]{:S(2)}, u32[]{:S(2)}) async-start(bf16[64,8,2048]{2,1,0:T(8,128)(2,1)} %fusion), calls=%async_computation.4 | async-start | bytes 4194304 | tf_op jit(solution)/shard_map/all_to_all | solution.py:170
  153.3 2.7 %convert_reduce_fusion = bf16[8,3,2048]{2,1,0:T(4,128)(2,1)S(1)} fusion(bf16[128,3,2048]{2,1,0:T(4,128)(2,1)} %all-to-all-done.2), kind=kLoop, calls=%fused_computation | loop fusion | flops 1523712 | bytes 1671168 | tf_op jit(solution)/shard_map/reduce_sum | solution.py:269
  156.0 25.5 %all-to-all-done.4 = bf16[64,8,2048]{2,1,0:T(8,128)(2,1)} async-done(((bf16[64,8,2048]{2,1,0:T(8,128)(2,1)}), bf16[64,8,2048]{2,1,0:T(8,128)(2,1)}, u32[]{:S(2)}, u32[]{:S(2)}) %all-to-all-start.4) | async-done | bytes 2097184 | tf_op jit(solution)/shard_map/all_to_all | solution.py:170
  181.5 1.9 %convert_reduce_fusion.1 = f32[8,2048]{1,0:T(8,128)S(1)} fusion(bf16[64,8,2048]{2,1,0:T(8,128)(2,1)} %all-to-all-done.4), kind=kLoop, calls=%fused_computation.1 | loop fusion | flops 2080768 | bytes 2162688 | tf_op jit(solution)/shard_map/reduce_sum | solution.py:171
  (50 shorter events, 6.6 us)
Async XLA Ops:
  0.6 88.7 %copy-start = (bf16[448,2048]{1,0:T(8,128)(2,1)S(1)}, bf16[448,2048]{1,0:T(8,128)(2,1)}, u32[]{:S(2)}) copy-start(bf16[448,2048]{1,0:T(8,128)(2,1)} %param.33) | copy-start | bytes 5505028
  0.6 2.3 %copy-start.1 = (bf16[2048,1024]{1,0:T(8,128)(2,1)S(1)}, bf16[2048,1024]{1,0:T(8,128)(2,1)}, u32[]{:S(2)}) copy-start(bf16[2048,1024]{1,0:T(8,128)(2,1)} %wq_h.1) | copy-start | bytes 12582916
  3.0 2.2 %copy-start.2 = (bf16[1024,2048]{1,0:T(8,128)(2,1)S(1)}, bf16[1024,2048]{1,0:T(8,128)(2,1)}, u32[]{:S(2)}) copy-start(bf16[1024,2048]{1,0:T(8,128)(2,1)} %wo_h.1) | copy-start | bytes 12582916
  5.2 2.2 %copy-start.3 = (bf16[16,1024,128]{2,1,0:T(8,128)(2,1)S(1)}, bf16[16,1024,128]{2,1,0:T(8,128)(2,1)}, u32[]{:S(2)}) copy-start(bf16[16,1024,128]{2,1,0:T(8,128)(2,1)} %ck_h.1) | copy-start | bytes 12582916
  7.3 1.0 copy-start.4
  8.4 1.0 copy-start.5
  9.4 0.8 copy-start.6
  10.3 0.7 copy-start.8
  11.0 0.7 copy-start.9
  11.6 0.7 copy-start.10
  12.3 18.8 %copy-start.16 = (s32[8,2]{0,1:T(2,128)S(1)}, s32[8,2]{0,1:T(2,128)}, u32[]{:S(2)}) copy-start(s32[8,2]{0,1:T(2,128)} %param.38) | copy-start | bytes 196
  12.3 19.8 %copy-start.7 = (bf16[16,2048]{1,0:T(8,128)(2,1)S(1)}, bf16[16,2048]{1,0:T(8,128)(2,1)}, u32[]{:S(2)}) copy-start(bf16[16,2048]{1,0:T(8,128)(2,1)} %tokens.1) | copy-start | bytes 196612
  12.3 20.2 %copy-start.14 = (f32[2048]{0:T(1024)S(1)}, f32[2048]{0:T(1024)}, u32[]{:S(2)}) copy-start(f32[2048]{0:T(1024)} %param.30) | copy-start | bytes 24580
  26.4 5.7 %all-to-all-start = ((bf16[2,8,2048]{2,1,0:T(8,128)(2,1)}), bf16[2,8,2048]{2,1,0:T(8,128)(2,1)S(1)}, u32[]{:S(2)}, u32[]{:S(2)}) async-start(bf16[2,8,2048]{2,1,0:T(8,128)(2,1)} %bitcast.2), calls=%async_computation | async-start | bytes 131072 | tf_op jit(solution)/shard_map/all_to_all | solution.py:170
  76.3 33.9 %all-to-all-start.3 = ((bf16[64,8,2048]{2,1,0:T(8,128)(2,1)}), bf16[64,8,2048]{2,1,0:T(8,128)(2,1)}, u32[]{:S(2)}, u32[]{:S(2)}) async-start(bf16[64,8,2048]{2,1,0:T(8,128)(2,1)} %broadcast_in_dim.28), calls=%async_computation.3 | async-start | bytes 4194304 | tf_op jit(solution)/shard_map/all_to_all | solution.py:176
  99.4 18.2 %copy-start.15 = (bf16[2048]{0:T(1024)(128)(2,1)S(1)}, bf16[2048]{0:T(1024)(128)(2,1)}, u32[]{:S(2)}) copy-start(bf16[2048]{0:T(1024)(128)(2,1)} %param.37) | copy-start | bytes 12292
  110.2 37.4 %all-to-all-start.2 = ((bf16[128,3,2048]{2,1,0:T(4,128)(2,1)}), bf16[128,3,2048]{2,1,0:T(4,128)(2,1)}, u32[]{:S(2)}, u32[]{:S(2)}) async-start(bf16[128,3,2048]{2,1,0:T(4,128)(2,1)} %convert_element_type.72), calls=%async_computation.2 | async-start | bytes 4194304 | tf_op jit(solution)/shard_map/all_to_all | solution.py:266
  117.5 2.4 %copy-start.13 = (bf16[2048,112]{0,1:T(8,128)(2,1)S(1)}, bf16[2048,112]{0,1:T(8,128)(2,1)}, u32[]{:S(2)}) copy-start(bf16[2048,112]{0,1:T(8,128)(2,1)} %param.34) | copy-start | bytes 1376260
  117.6 4.8 %copy-start.11 = (bf16[112,2048]{1,0:T(8,128)(2,1)S(1)}, bf16[112,2048]{1,0:T(8,128)(2,1)}, u32[]{:S(2)}) copy-start(bf16[112,2048]{1,0:T(8,128)(2,1)} %param.36) | copy-start | bytes 1376260
  117.6 4.8 %copy-start.12 = (bf16[2048,112]{0,1:T(8,128)(2,1)S(1)}, bf16[2048,112]{0,1:T(8,128)(2,1)}, u32[]{:S(2)}) copy-start(bf16[2048,112]{0,1:T(8,128)(2,1)} %param.35) | copy-start | bytes 1376260
  126.9 26.4 %copy-start.17 = (bf16[8,2]{0,1:T(2,128)(2,1)S(1)}, bf16[8,2]{0,1:T(2,128)(2,1)}, u32[]{:S(2)}) copy-start(bf16[8,2]{0,1:T(2,128)(2,1)} %param.39) | copy-start | bytes 100
  147.6 33.9 %all-to-all-start.4 = ((bf16[64,8,2048]{2,1,0:T(8,128)(2,1)}), bf16[64,8,2048]{2,1,0:T(8,128)(2,1)}, u32[]{:S(2)}, u32[]{:S(2)}) async-start(bf16[64,8,2048]{2,1,0:T(8,128)(2,1)} %fusion), calls=%async_computation.4 | async-start | bytes 4194304 | tf_op jit(solution)/shard_map/all_to_all | solution.py:170
